TPU v7x, 32 devices: a whole 2x2x4 slice. The times are simulated.
32 devices in a mesh: sp: 16 (over z, y, x), tp: 2 (over core).
Axes of the slice: x: 2, y: 2, z: 4, core: 2. Of those that a mesh axis runs over, the one named last changes fastest.
Arguments:
- latent: bfloat16 [4096, 2048], P('sp'), may hold values from -6 to 6
- context: bfloat16 [512, 2048], P('sp'), may hold values from -6 to 6
- cond: bfloat16 [2048], P('sp'), may hold values from -6 to 6
- cond_ctx: bfloat16 [2048], P('sp'), may hold values from -6 to 6
- shift_weight: bfloat16 [2048, 2048], P('sp', 'tp'), may hold values from -0.125 to 0.125
- scale_weight: bfloat16 [2048, 2048], P('sp', 'tp'), may hold values from -0.125 to 0.125
- gate_weight: bfloat16 [2048, 2048], P('sp', 'tp'), may hold values from -0.25 to 0.25
- norm_gain: bfloat16 [2048], replicated, may hold values from 0.099609375 to 1.8984375
- query_weight: bfloat16 [2048, 1024], P(None, 'tp'), may hold values from -0.125 to 0.125
- key_weight: bfloat16 [2048, 1024], P(None, 'tp'), may hold values from -0.125 to 0.125
- value_weight: bfloat16 [2048, 1024], P(None, 'tp'), may hold values from -0.125 to 0.125
- query_gain: bfloat16 [64], replicated, may hold values from 0.099609375 to 1.8984375
- key_gain: bfloat16 [64], replicated, may hold values from 0.099609375 to 1.8984375
- offset_bias: float32 [16, 15, 31], P('tp'), may hold values from -0.5 to 251
- out_weight: bfloat16 [1024, 2048], P(None, 'tp'), may hold values from -1.5 to 1.5
Outputs:
- updated: bfloat16 [4096, 2048], P('sp', 'tp')
All inputs are finite; a program needn't handle non-finite values.
Results may differ from a plain program's by a relative error of at most 0.0077.
Values may be sent and summed in bfloat16 or wider, within the bound.
A program may use at most 128 MiB of HBM per device.

v0:
```python
import functools

import jax
import jax.numpy as jnp
import numpy as np
from jax import lax
from jax.experimental import pallas as pl
from jax.experimental.pallas import tpu as pltpu
from jax.sharding import PartitionSpec as P

HEAD_DIM = 64
WIN_ROWS = 8
WIN_COLS = 16
GRID_W = 64


EPS = 1e-06


def padded_2(block, sides, width):
    for axis, dim in sides:
        count = lax.axis_size(axis)
        forward = [(i, i + 1) for i in range(count - 1)]
        backward = [(target, source) for source, target in forward]
        low = lax.ppermute(
            lax.slice_in_dim(block, block.shape[dim] - width, None, axis=dim), axis, forward
        )
        high = lax.ppermute(lax.slice_in_dim(block, 0, width, axis=dim), axis, backward)
        block = jnp.concatenate([low, block, high], axis=dim)
    return block


def modulate(rows, norm_gain, scale, shift):
    values = rows.astype(jnp.float32)
    normed = values * lax.rsqrt(jnp.mean(values * values, axis=-1, keepdims=True) + EPS)
    return (normed * norm_gain.astype(jnp.float32) * (1.0 + scale) + shift).astype(jnp.bfloat16)


def project_heads(hidden, weight, gain):
    raw = jnp.dot(hidden, weight, preferred_element_type=jnp.float32)
    split = raw.reshape(hidden.shape[0], -1, HEAD_DIM)
    if gain is None:
        return split.astype(jnp.bfloat16)
    normed = split * lax.rsqrt(jnp.mean(split * split, axis=-1, keepdims=True) + EPS)
    return (normed * gain.astype(jnp.float32)).astype(jnp.bfloat16)


def body(
    latent,
    context,
    cond,
    cond_ctx,
    shift_weight,
    scale_weight,
    gate_weight,
    norm_gain,
    query_weight,
    key_weight,
    value_weight,
    query_gain,
    key_gain,
    offset_bias,
    out_weight,
):
    width = latent.shape[1]
    col_width = shift_weight.shape[1]
    tp_offset = lax.axis_index("tp") * col_width
    act = jax.nn.silu(cond.astype(jnp.float32)).astype(jnp.bfloat16)
    act_ctx = jax.nn.silu(cond_ctx.astype(jnp.float32)).astype(jnp.bfloat16)
    acts = jnp.stack([act, act_ctx])
    terms = jnp.concatenate(
        [
            jnp.dot(acts, shift_weight, preferred_element_type=jnp.float32),
            jnp.dot(acts, scale_weight, preferred_element_type=jnp.float32),
            jnp.dot(acts[:1], gate_weight, preferred_element_type=jnp.float32),
        ],
        axis=0,
    )
    placed = lax.dynamic_update_slice_in_dim(
        jnp.zeros((5, width), jnp.float32), terms, tp_offset, 1
    )
    full = lax.psum(placed, ("sp", "tp"))
    shift, shift_ctx, scale, scale_ctx, gate = (full[0], full[1], full[2], full[3], full[4])
    heads_dev = offset_bias.shape[0]
    lane = heads_dev * HEAD_DIM
    all_rows = lax.all_gather(context, "sp", axis=0, tiled=True)
    hidden_ctx = modulate(all_rows, norm_gain, scale_ctx, shift_ctx)
    ctx_keys = project_heads(hidden_ctx, key_weight, key_gain)
    ctx_values = project_heads(hidden_ctx, value_weight, None)
    hidden = modulate(latent, norm_gain, scale, shift)
    queries = project_heads(hidden, query_weight, query_gain)
    keys = project_heads(hidden, key_weight, key_gain)
    values = project_heads(hidden, value_weight, None)
    rows_dev = latent.shape[0] // GRID_W
    reach = WIN_ROWS // 2
    grid_kv = jnp.stack(
        [keys.reshape(rows_dev, GRID_W, lane), values.reshape(rows_dev, GRID_W, lane)], axis=1
    )
    padded = padded_2(grid_kv, (("sp", 0),), reach)
    total_rows = rows_dev * lax.axis_size("sp")
    base = lax.axis_index("sp") * rows_dev
    local_rows = base + jnp.arange(rows_dev, dtype=jnp.int32)
    first = jnp.clip(local_rows - reach, 0, total_rows - WIN_ROWS)
    window_rows = jnp.arange(WIN_ROWS, dtype=jnp.int32)
    band_index = (first - base + reach)[:, None] + window_rows[None, :]
    band = jnp.take(padded, band_index, axis=0)
    n_blocks = GRID_W // WIN_COLS
    span = 2 * WIN_COLS
    starts = [
        min(max(block * WIN_COLS - WIN_COLS // 2, 0), GRID_W - span) for block in range(n_blocks)
    ]
    blocked = jnp.stack([band[:, :, :, begin : begin + span] for begin in starts], axis=3)
    blocked = blocked.reshape(rows_dev, WIN_ROWS, 2, n_blocks, span, heads_dev, HEAD_DIM)
    key_blocks = blocked[:, :, 0]
    value_blocks = blocked[:, :, 1]
    query_col = np.arange(n_blocks)[:, None, None] * WIN_COLS + np.arange(WIN_COLS)[None, :, None]
    key_col = np.array(starts)[:, None, None] + np.arange(span)[None, None, :]
    window_first = np.clip(query_col - WIN_COLS // 2, 0, GRID_W - WIN_COLS)
    inside = (key_col >= window_first) & (key_col < window_first + WIN_COLS)
    col_offset = np.clip(key_col - query_col + WIN_COLS - 1, 0, 2 * WIN_COLS - 2)
    col_onehot = (col_offset[..., None] == np.arange(2 * WIN_COLS - 1)).astype(np.float32)
    row_offset = first[:, None] + window_rows[None, :] - local_rows[:, None] + WIN_ROWS - 1
    row_onehot = (row_offset[..., None] == jnp.arange(2 * WIN_ROWS - 1, dtype=jnp.int32)).astype(
        jnp.float32
    )
    by_col = jnp.einsum(
        "hxc,bqkc->hxbqk", offset_bias, jnp.asarray(col_onehot), precision=lax.Precision.HIGHEST
    )
    bias = jnp.einsum("rjx,hxbqk->rhbqjk", row_onehot, by_col, precision=lax.Precision.HIGHEST)
    factor = HEAD_DIM ** (-0.5)
    grid_q = queries.reshape(rows_dev, n_blocks, WIN_COLS, heads_dev, HEAD_DIM)
    local_scores = (
        jnp.einsum("rbqhd,rjbkhd->rhbqjk", grid_q, key_blocks, preferred_element_type=jnp.float32)
        * factor
    )
    local_scores = jnp.where(jnp.asarray(inside)[:, :, None, :], local_scores + bias, -jnp.inf)
    band_len = WIN_ROWS * span
    local_scores = local_scores.reshape(rows_dev, heads_dev, n_blocks, WIN_COLS, band_len)
    ctx_scores = (
        jnp.einsum("rbqhd,chd->rhbqc", grid_q, ctx_keys, preferred_element_type=jnp.float32)
        * factor
    )
    scores = jnp.concatenate([local_scores, ctx_scores], axis=-1)
    top = jnp.max(scores, axis=-1, keepdims=True)
    expd = jnp.exp(scores - top)
    weights = (expd / jnp.sum(expd, axis=-1, keepdims=True)).astype(jnp.bfloat16)
    local_w = weights[..., :band_len].reshape(
        rows_dev, heads_dev, n_blocks, WIN_COLS, WIN_ROWS, span
    )
    mixed = jnp.einsum(
        "rhbqjk,rjbkhd->rbqhd", local_w, value_blocks, preferred_element_type=jnp.float32
    )
    mixed = mixed + jnp.einsum(
        "rhbqc,chd->rbqhd", weights[..., band_len:], ctx_values, preferred_element_type=jnp.float32
    )
    mixed = mixed.astype(jnp.bfloat16).reshape(latent.shape[0], lane)
    projected = jnp.dot(
        lax.all_gather(mixed, "tp", axis=1, tiled=True),
        out_weight,
        preferred_element_type=jnp.float32,
    )
    own_cols = lax.dynamic_slice_in_dim(latent, tp_offset, col_width, 1).astype(jnp.float32)
    gate_cols = lax.dynamic_slice_in_dim(gate, tp_offset, col_width, 0)
    return (own_cols + gate_cols[None, :] * projected).astype(jnp.bfloat16)


LANES = 128
NEG = -1e30


def head_norm(raw, gain, ones):
    square = raw * raw
    high = square.astype(jnp.bfloat16)
    low = (square - high.astype(jnp.float32)).astype(jnp.bfloat16)
    parts = []
    for begin in range(0, raw.shape[1], LANES):
        cut = slice(begin, begin + LANES)
        parts.append(
            jnp.dot(high[:, cut], ones, preferred_element_type=jnp.float32)
            + jnp.dot(low[:, cut], ones, preferred_element_type=jnp.float32)
        )
    mean = jnp.concatenate(parts, axis=1) * (1.0 / HEAD_DIM)
    return raw * lax.rsqrt(mean + EPS) * gain


def attend_kernel(
    total_rows,
    low_ref,
    own_ref,
    high_ref,
    ctx_ref,
    mod_ref,
    norm_gain_ref,
    wq_ref,
    wk_ref,
    wv_ref,
    query_gain_ref,
    key_gain_ref,
    table_ref,
    out_ref,
    q_buf,
    k_buf,
    v_buf,
    ck_buf,
    cv_buf,
    low_vmem,
    own_vmem,
    high_vmem,
    ctx_vmem,
    wq_vmem,
    wk_vmem,
    wv_vmem,
    sems,
):
    tokens, lane = out_ref.shape
    streams = {}
    for place, (name, source, target) in enumerate(
        (
            ("own", own_ref, own_vmem),
            ("wk", wk_ref, wk_vmem),
            ("wv", wv_ref, wv_vmem),
            ("wq", wq_ref, wq_vmem),
            ("low", low_ref, low_vmem),
            ("high", high_ref, high_vmem),
            ("ctx", ctx_ref, ctx_vmem),
        )
    ):
        streams[name] = pltpu.make_async_copy(source, target, sems.at[place])
        streams[name].start()
    rows_dev = tokens // GRID_W
    reach = WIN_ROWS // 2
    halo = reach * GRID_W
    heads = lane // HEAD_DIM
    norm_gain = norm_gain_ref[...].astype(jnp.float32)
    half = lax.broadcasted_iota(jnp.int32, (LANES, LANES), 0) // HEAD_DIM
    half_t = lax.broadcasted_iota(jnp.int32, (LANES, LANES), 1) // HEAD_DIM
    ones = (half == half_t).astype(jnp.float32).astype(jnp.bfloat16)
    query_gain = jnp.concatenate([query_gain_ref[...].astype(jnp.float32)] * heads, axis=1)
    key_gain = jnp.concatenate([key_gain_ref[...].astype(jnp.float32)] * heads, axis=1)

    def hidden_of(x, shift, scale):
        values = x.astype(jnp.float32)
        inv = lax.rsqrt(jnp.mean(values * values, axis=-1, keepdims=True) + EPS)
        return (values * inv * (norm_gain * (1.0 + scale)) + shift).astype(jnp.bfloat16)

    def keys_values(hidden, k_out, v_out, at):
        raw = jnp.dot(hidden, wk_vmem[...], preferred_element_type=jnp.float32)
        k_out[pl.ds(at, hidden.shape[0]), :] = head_norm(raw, key_gain, ones).astype(jnp.bfloat16)
        v_out[pl.ds(at, hidden.shape[0]), :] = jnp.dot(
            hidden, wv_vmem[...], preferred_element_type=jnp.float32
        ).astype(jnp.bfloat16)

    shift, shift_ctx = mod_ref[0:1, :], mod_ref[1:2, :]
    scale, scale_ctx = mod_ref[2:3, :], mod_ref[3:4, :]
    step = min(256, tokens)
    streams["own"].wait()
    for begin in range(0, tokens, step):
        hidden = hidden_of(own_vmem[begin : begin + step, :], shift, scale)
        if begin == 0:
            streams["wk"].wait()
            streams["wv"].wait()
        keys_values(hidden, k_buf, v_buf, halo + begin)
        if begin == 0:
            streams["wq"].wait()
        raw = jnp.dot(hidden, wq_vmem[...], preferred_element_type=jnp.float32)
        q_buf[begin : begin + step, :] = (
            head_norm(raw, query_gain, ones).astype(jnp.bfloat16) * HEAD_DIM ** (-0.5)
        ).astype(jnp.bfloat16)
    streams["low"].wait()
    keys_values(hidden_of(low_vmem[...], shift, scale), k_buf, v_buf, 0)
    streams["high"].wait()
    keys_values(hidden_of(high_vmem[...], shift, scale), k_buf, v_buf, halo + tokens)
    ctx_step = min(256, ctx_vmem.shape[0])
    streams["ctx"].wait()

    @pl.loop(0, ctx_vmem.shape[0] // ctx_step)
    def _(block):
        at = pl.multiple_of(block * ctx_step, ctx_step)
        hidden = hidden_of(ctx_vmem[pl.ds(at, ctx_step), :], shift_ctx, scale_ctx)
        keys_values(hidden, ck_buf, cv_buf, at)

    base = lax.axis_index("sp") * rows_dev
    query_col = lax.broadcasted_iota(jnp.int32, (GRID_W, LANES), 0)
    lane_at = lax.broadcasted_iota(jnp.int32, (GRID_W, LANES), 1)
    key_col = lane_at % GRID_W
    window_first = jnp.clip(query_col - WIN_COLS // 2, 0, GRID_W - WIN_COLS)
    inside = (key_col >= window_first) & (key_col < window_first + WIN_COLS)
    first_head = lane_at < HEAD_DIM
    per_tile = LANES // GRID_W
    contract = (((1,), (1,)), ((), ()))

    @pl.loop(0, lane // LANES)
    def _(pair):
        cols = pl.ds(pl.multiple_of(pair * LANES, LANES), LANES)
        for row in range(rows_dev):
            first = jnp.clip(base + row - reach, 0, total_rows - WIN_ROWS)
            begin = pl.multiple_of((first - base + reach) * GRID_W, GRID_W)
            offset = first - base - row + WIN_ROWS - 1
            mine = slice(row * GRID_W, (row + 1) * GRID_W)
            query = q_buf[mine, cols]
            zero = jnp.zeros_like(query)
            query2 = jnp.concatenate(
                [jnp.where(first_head, query, zero), jnp.where(first_head, zero, query)], axis=0
            )
            band = pl.ds(begin, WIN_ROWS * GRID_W)
            local = lax.dot_general(
                query2, k_buf[band, cols], contract, preferred_element_type=jnp.float32
            )
            ctx = lax.dot_general(
                query2, ck_buf[:, cols], contract, preferred_element_type=jnp.float32
            )
            biases = []
            for head in range(2):
                tiles = []
                for tile in range(WIN_ROWS // per_tile):
                    entry = (pair * 2 + head) * (2 * WIN_ROWS) + offset + tile * per_tile
                    line = jnp.broadcast_to(table_ref[entry], (GRID_W, LANES))
                    moved = pltpu.roll(line, LANES - (WIN_COLS - 1), 1, stride=1, stride_axis=0)
                    tiles.append(jnp.where(inside, moved, NEG))
                biases.append(jnp.concatenate(tiles, axis=1))
            local = local + jnp.concatenate(biases, axis=0)
            top = jnp.maximum(
                jnp.max(local, axis=-1, keepdims=True), jnp.max(ctx, axis=-1, keepdims=True)
            )
            local = jnp.exp(local - top)
            ctx = jnp.exp(ctx - top)
            total = jnp.sum(local, axis=-1, keepdims=True) + jnp.sum(ctx, axis=-1, keepdims=True)
            mixed = jnp.dot(
                local.astype(jnp.bfloat16), v_buf[band, cols], preferred_element_type=jnp.float32
            ) + jnp.dot(
                ctx.astype(jnp.bfloat16), cv_buf[:, cols], preferred_element_type=jnp.float32
            )
            mixed = mixed / total
            out_ref[mine, cols] = jnp.where(
                first_head, mixed[:GRID_W], mixed[GRID_W:]
            ).astype(jnp.bfloat16)


def bias_lines(offset_bias):
    heads = offset_bias.shape[0]
    wide = jnp.pad(offset_bias, ((0, 0), (0, 2), (0, GRID_W - offset_bias.shape[2])))
    lines = jnp.concatenate([wide[:, :-1], wide[:, 1:]], axis=2)
    return lines.reshape(heads * 2 * WIN_ROWS, 1, LANES)


def attend(
    low, own, high, ctx, mod, norm_gain, wq, wk, wv, query_gain, key_gain, offset_bias, total_rows
):
    tokens, lane = own.shape[0], wq.shape[1]
    halo = low.shape[0]
    rows = tokens + 2 * halo
    vmem = pl.BlockSpec(memory_space=pltpu.VMEM)
    hbm = pl.BlockSpec(memory_space=pl.ANY)
    return pl.pallas_call(
        functools.partial(attend_kernel, total_rows),
        out_shape=jax.ShapeDtypeStruct((tokens, lane), jnp.bfloat16),
        in_specs=[hbm] * 4 + [vmem] * 2 + [hbm] * 3 + [vmem] * 3,
        out_specs=vmem,
        scratch_shapes=[
            pltpu.VMEM((tokens, lane), jnp.bfloat16),
            pltpu.VMEM((rows, lane), jnp.bfloat16),
            pltpu.VMEM((rows, lane), jnp.bfloat16),
            pltpu.VMEM((ctx.shape[0], lane), jnp.bfloat16),
            pltpu.VMEM((ctx.shape[0], lane), jnp.bfloat16),
        ]
        + [pltpu.VMEM(x.shape, x.dtype) for x in (low, own, high, ctx, wq, wk, wv)]
        + [pltpu.SemaphoreType.DMA((7,))],
        cost_estimate=pl.CostEstimate(
            flops=12 * tokens * own.shape[1] * lane, bytes_accessed=1 << 24, transcendentals=1 << 21
        ),
        name="attend",
    )(
        low, own, high, ctx, mod,
        norm_gain[None, :],
        wq, wk, wv,
        query_gain[None, :],
        key_gain[None, :],
        bias_lines(offset_bias),
    )


def bit_flip(index, bit):
    return index + bit - 2 * bit * ((index // bit) % 2)


def exchange_kernel(
    bits,
    tp_size,
    cond_ref,
    cond_ctx_ref,
    shift_ref,
    scale_ref,
    gate_ref,
    latent_ref,
    context_ref,
    mod_ref,
    low_ref,
    high_ref,
    ctx_ref,
    sums,
    arrived,
    local_sem,
    mod_send,
    mod_recv,
    ctx_send,
    ctx_recv,
    halo_send,
    halo_recv,
    tp_send,
    tp_recv,
):
    me = lax.axis_index("sp")
    mine = lax.axis_index("tp")
    size = lax.axis_size("sp")
    mesh_ids = pl.DeviceIdType.MESH
    barrier = pltpu.get_barrier_semaphore()
    for bit in bits:
        pl.semaphore_signal(
            barrier, inc=1, device_id={"sp": bit_flip(me, bit)}, device_id_type=mesh_ids
        )
    for away in range(1, tp_size):
        pl.semaphore_signal(
            barrier, inc=1, device_id={"tp": (mine + away) % tp_size}, device_id_type=mesh_ids
        )

    for away in (1, size - 1):
        pl.semaphore_signal(
            barrier, inc=1, device_id={"sp": (me + away) % size}, device_id_type=mesh_ids
        )

    share = latent_ref.shape[1] // tp_size
    cols = pl.ds(pl.multiple_of(mine * share, share), share)
    block = context_ref.shape[0]

    def rows_of(mask):
        index = me
        for bit in bits:
            if mask & bit:
                index = bit_flip(index, bit)
        return pl.ds(pl.multiple_of(index * block, block), block)

    keep = pltpu.make_async_copy(
        context_ref.at[:, cols], ctx_ref.at[rows_of(0), cols], local_sem.at[0]
    )
    keep.start()

    def silu(ref):
        v = ref[...].astype(jnp.float32)
        return (v / (1.0 + jnp.exp(-v))).astype(jnp.bfloat16)

    acts = jnp.concatenate([silu(cond_ref), silu(cond_ctx_ref)], axis=0)
    f32 = jnp.float32
    sums[0, 0:2, :] = jnp.dot(acts, shift_ref[...], preferred_element_type=f32)
    sums[0, 2:4, :] = jnp.dot(acts, scale_ref[...], preferred_element_type=f32)
    sums[0, 4:5, :] = jnp.dot(acts, gate_ref[...], preferred_element_type=f32)[0:1]

    pl.semaphore_wait(barrier, len(bits) + tp_size + 1)

    def remote(source, target, send, recv, where):
        return pltpu.make_async_remote_copy(
            src_ref=source, dst_ref=target, send_sem=send, recv_sem=recv,
            device_id=where, device_id_type=mesh_ids,
        )

    tokens = latent_ref.shape[0]
    halo = low_ref.shape[0]
    up = remote(
        latent_ref.at[pl.ds(tokens - halo, halo), cols], low_ref.at[:, cols],
        halo_send.at[0], halo_recv.at[0], {"sp": me + 1},
    )
    down = remote(
        latent_ref.at[pl.ds(0, halo), cols], high_ref.at[:, cols],
        halo_send.at[1], halo_recv.at[1], {"sp": me - 1},
    )
    keep.wait()
    held = [0]
    pending = {}
    started = []
    count = 0
    for step, bit in enumerate(bits):
        where = {"sp": bit_flip(me, bit)}
        term = remote(
            sums.at[step], arrived.at[step], mod_send.at[step], mod_recv.at[step], where
        )
        term.start()
        for mask in list(held):
            if mask in pending:
                pending.pop(mask).wait_recv()
            place = ctx_ref.at[rows_of(mask), cols]
            copy = remote(place, place, ctx_send.at[count], ctx_recv.at[count], where)
            copy.start()
            started.append(copy)
            pending[mask | bit] = remote(
                ctx_ref.at[rows_of(mask | bit), cols], ctx_ref.at[rows_of(mask | bit), cols],
                ctx_send.at[count], ctx_recv.at[count], where,
            )
            held.append(mask | bit)
            count += 1
        if step == 0:

            @pl.when(me < size - 1)
            def _():
                up.start()

            @pl.when(me > 0)
            def _():
                down.start()

        term.wait()
        sums[step + 1] = sums[step] + arrived[step]

    width = sums.shape[2]
    own = pl.ds(pl.multiple_of(mine * width, width), width)
    mod_ref[:, own] = sums[len(bits)]

    def spread(place, slot):
        copies = []
        for away in range(1, tp_size):
            at = slot * (tp_size - 1) + away - 1
            copies.append(
                remote(
                    place, place, tp_send.at[at], tp_recv.at[at], {"tp": (mine + away) % tp_size}
                )
            )
        for copy in copies:
            copy.start()

    def finish(ref, span, slot):
        for away in range(1, tp_size):
            at = slot * (tp_size - 1) + away - 1
            source = (mine + tp_size - away) % tp_size
            came = ref.at[:, pl.ds(pl.multiple_of(source * span, span), span)]
            wait = remote(came, came, tp_send.at[at], tp_recv.at[at], {"tp": source})
            wait.wait_send()
            wait.wait_recv()

    spread(mod_ref.at[:, own], 0)

    @pl.when(me > 0)
    def _():
        up.wait_recv()
        spread(low_ref.at[:, cols], 1)

    @pl.when(me < size - 1)
    def _():
        down.wait_recv()
        spread(high_ref.at[:, cols], 2)

    for mask in list(pending):
        pending.pop(mask).wait_recv()
    spread(ctx_ref.at[:, cols], 3)
    for copy in started:
        copy.wait_send()

    @pl.when(me < size - 1)
    def _():
        up.wait_send()

    @pl.when(me > 0)
    def _():
        down.wait_send()

    finish(mod_ref, width, 0)

    @pl.when(me > 0)
    def _():
        finish(low_ref, share, 1)

    @pl.when(me < size - 1)
    def _():
        finish(high_ref, share, 2)

    finish(ctx_ref, share, 3)


def doubling_order(size):
    bits = [1 << k for k in range(size.bit_length() - 1)]
    return tuple(bits[:1] + bits[:0:-1])


def exchange(latent, context, cond, cond_ctx, shift_weight, scale_weight, gate_weight):
    size, tp_size = lax.axis_size("sp"), lax.axis_size("tp")
    bits = doubling_order(size)
    width = latent.shape[1]
    col_width = shift_weight.shape[1]
    halo = WIN_ROWS // 2 * GRID_W
    vmem = pl.BlockSpec(memory_space=pltpu.VMEM)
    hbm = pl.BlockSpec(memory_space=pl.ANY)
    dma = pltpu.SemaphoreType.DMA
    tp_copies = max(4 * (tp_size - 1), 1)
    f32 = jnp.float32
    return pl.pallas_call(
        functools.partial(exchange_kernel, bits, tp_size),
        out_shape=[
            jax.ShapeDtypeStruct((5, width), f32),
            jax.ShapeDtypeStruct((halo, width), latent.dtype),
            jax.ShapeDtypeStruct((halo, width), latent.dtype),
            jax.ShapeDtypeStruct((context.shape[0] * size, width), context.dtype),
        ],
        in_specs=[vmem] * 5 + [hbm] * 2,
        out_specs=[vmem] * 4,
        scratch_shapes=[
            pltpu.VMEM((len(bits) + 1, 5, col_width), f32),
            pltpu.VMEM((len(bits), 5, col_width), f32),
            dma((1,)),
            dma((len(bits),)),
            dma((len(bits),)),
            dma((size,)),
            dma((size,)),
            dma((2,)),
            dma((2,)),
            dma((tp_copies,)),
            dma((tp_copies,)),
        ],
        compiler_params=pltpu.CompilerParams(collective_id=0, has_side_effects=True),
        name="exchange",
    )(cond[None, :], cond_ctx[None, :], shift_weight, scale_weight, gate_weight, latent, context)


def fast_body(
    latent, context, cond, cond_ctx, shift_weight, scale_weight, gate_weight, norm_gain,
    query_weight, key_weight, value_weight, query_gain, key_gain, offset_bias, out_weight,
):
    col_width = shift_weight.shape[1]
    tp_offset = lax.axis_index("tp") * col_width
    mod, low, high, all_ctx = exchange(
        latent, context, cond, cond_ctx, shift_weight, scale_weight, gate_weight
    )
    total_rows = (latent.shape[0] // GRID_W) * lax.axis_size("sp")
    mixed = attend(
        low, latent, high, all_ctx, mod, norm_gain, query_weight, key_weight, value_weight,
        query_gain, key_gain, offset_bias, total_rows,
    )
    projected = jnp.dot(
        lax.all_gather(mixed, "tp", axis=1, tiled=True),
        out_weight,
        preferred_element_type=jnp.float32,
    )
    own_cols = lax.dynamic_slice_in_dim(latent, tp_offset, col_width, 1).astype(jnp.float32)
    gate_cols = lax.dynamic_slice_in_dim(mod[4], tp_offset, col_width, 0)
    return (own_cols + gate_cols[None, :] * projected).astype(jnp.bfloat16)


def choose(latent, context, *rest):
    rows_dev = latent.shape[0] // GRID_W
    lane = rest[6].shape[1]
    size = lax.axis_size("sp")
    fits = size >= 4 and size & (size - 1) == 0 and context.shape[0] % 8 == 0
    if fits and lane % LANES == 0 and rows_dev >= WIN_ROWS // 2 and 2 * GRID_W == LANES:
        return fast_body(latent, context, *rest)
    return body(latent, context, *rest)


def solution(mesh):
    in_specs = (
        P("sp", None),
        P("sp", None),
        P("sp"),
        P("sp"),
        P("sp", "tp"),
        P("sp", "tp"),
        P("sp", "tp"),
        P(),
        P(None, "tp"),
        P(None, "tp"),
        P(None, "tp"),
        P(),
        P(),
        P("tp", None, None),
        P(None, "tp"),
    )
    out_specs = P("sp", "tp")
    return jax.shard_map(choose, mesh=mesh, in_specs=in_specs, out_specs=out_specs, check_vma=False)
```

profile of v0, /device:TPU:3, one launch (start us, length us, event | category | flops | bytes accessed | tf_op | source)
XLA Modules:
  0.0 77.1 jit_solution(1502280432348257472)
XLA Ops:
  0.0 0.0 copy-start
  0.0 0.0 copy-start.2
  0.0 47.6 %exchange.1 = (f32[5,2048]{1,0:T(8,128)}, bf16[256,2048]{1,0:T(8,128)(2,1)}, bf16[256,2048]{1,0:T(8,128)(2,1)}, bf16[512,2048]{1,0:T(8,128)(2,1)}) custom-call(bf16[1,128]{1,0:T(2,128)(2,1)} %bitcast.10, bf16[1,128]{1,0:T(2,128)(2,1)} %bitcast.11, bf16[128,1024]{1,0:T(8,128)(2,1)} %shift_ref.1, bf16[128,1024]{1,0:T(8,128)(2,1)} %scale_ref.1, ...), custom_call_target="tpu_custom_call" | custom-call | tf_op jit(solution)/shard_map/exchange/pallas_call | solution.py:592
  47.6 0.9 %pad_slice_fusion.1 = (f32[8,16,64]{2,0,1:T(8,128)S(1)}, f32[8,16,64]{2,0,1:T(8,128)S(1)}) fusion(f32[8,15,31]{2,0,1:T(8,128)} %param.28), kind=kLoop, calls=%fused_computation.4 | loop fusion | bytes 80416 | tf_op jit(solution)/shard_map/slice | solution.py:342
  48.5 0.1 pad_maximum_fusion
  48.6 0.6 copy.16
  49.2 0.0 copy-done.2
  49.2 0.6 broadcast_in_dim.18.norm_gain_ref
  49.8 0.0 copy-start.1
  49.8 19.9 %attend.1 = bf16[256,512]{1,0:T(8,128)(2,1)} custom-call(bf16[256,2048]{1,0:T(8,128)(2,1)} %get-tuple-element.10.low_ref, bf16[256,2048]{1,0:T(8,128)(2,1)} %own_ref.1, bf16[256,2048]{1,0:T(8,128)(2,1)} %get-tuple-element.11.high_ref, bf16[512,2048]{1,0:T(8,128)(2,1)} %get-tuple-element.12.ctx_ref, f32[5,2048]{1,0:T(8,128)} %get-tuple-element.9.mod_ref, ...), custom_call_target="tpu_custom_call" | custom-call | flops 3221225472 | bytes 16777216 | tf_op jit(solution)/shard_map/attend/pallas_call | solution.py:354
  69.8 3.8 %all_gather.3 = bf16[256,1024]{1,0:T(8,128)(2,1)} all-gather(bf16[256,512]{1,0:T(8,128)(2,1)} %attend.1), channel_id=1, replica_groups=mesh['sp'=16,'tp'=2] {'tp'}, dimensions={1}, use_global_device_ids=true | all-gather | bytes 786432 | tf_op jit(solution)/shard_map/all_gather | solution.py:635
  73.6 0.8 %slice.9 = f32[1,2048]{1,0:T(1,128)S(1)} slice(f32[5,2048]{1,0:T(8,128)} %get-tuple-element.9.mod_ref), slice={[4:5], [0:2048]} | slice | bytes 16384 | tf_op jit(solution)/shard_map/slice | solution.py:640
  74.5 0.0 copy-done
  74.5 0.0 copy-done.1
  74.5 2.6 %fusion.1 = bf16[256,1024]{1,0:T(8,128)(2,1)} fusion(bf16[256,1024]{1,0:T(8,128)(2,1)} %all_gather.3, bf16[1024,1024]{1,0:T(8,128)(2,1)S(1)} %copy-done, f32[1024]{0:T(1024)S(1)} %bitcast.9, bf16[256,2048]{1,0:T(8,128)(2,1)S(1)} %copy-done.1, s32[]{:T(128)S(6)} %select_n.4), kind=kOutput, calls=%fused_computation.2 | convolution fusion | flops 537919488 | bytes 3674116 | tf_op jit(solution)/shard_map/dot_general | solution.py:634
  (1 shorter events, 0.0 us)
Async XLA Ops:
  0.0 74.5 %copy-start = (bf16[1024,1024]{1,0:T(8,128)(2,1)S(1)}, bf16[1024,1024]{1,0:T(8,128)(2,1)}, u32[]{:S(2)}) copy-start(bf16[1024,1024]{1,0:T(8,128)(2,1)} %param.29) | copy-start | bytes 6291460
  0.0 49.2 %copy-start.2 = (bf16[2048]{0:T(1024)(128)(2,1)S(1)}, bf16[2048]{0:T(1024)(128)(2,1)}, u32[]{:S(2)}) copy-start(bf16[2048]{0:T(1024)(128)(2,1)} %param.22) | copy-start | bytes 12292
  49.8 24.7 %copy-start.1 = (bf16[256,2048]{1,0:T(8,128)(2,1)S(1)}, bf16[256,2048]{1,0:T(8,128)(2,1)}, u32[]{:S(2)}) copy-start(bf16[256,2048]{1,0:T(8,128)(2,1)} %own_ref.1) | copy-start | bytes 3145732
where the time goes:
time: 77.4 us; the launch traced here: 77.1 us
  Pallas kernels  67.5 us (87%)
  blocking collectives  3.84 us (5%)
  local copies, waits for them, and re-layouts  3.01 us (4%)
  matrix products  2.56 us (3%)
    pallas_call x1, Pallas kernels, exchange(): pl.pallas_call(functools.partial(exchange_kernel, bits, tp_size), out_sha...  47.6 us
    pallas_call x1, Pallas kernels, attend(): pl.pallas_call(functools.partial(attend_kernel, total_rows), out_shape=ja...  19.9 us
    all_gather x1, blocking collectives, fast_body(): lax.all_gather(mixed, 'tp', axis=1, tiled=True)  3.84 us
    dot_general x1, matrix products, fast_body(): jnp.dot(lax.all_gather(mixed, 'tp', axis=1, tiled=True), out_weight, pref...  2.56 us

commit v1 on v0

--- a/solution.py
+++ b/solution.py
@@ -641,12 +641,507 @@
     return (own_cols + gate_cols[None, :] * projected).astype(jnp.bfloat16)
 
 
+LOG2E = 1.4426950408889634
+
+
+def fused_kernel(
+    total_rows,
+    latent_ref, context_ref, cond_ref, cond_ctx_ref, shift_ref, scale_ref, gate_ref,
+    norm_gain_ref, wq_ref, wk_ref, wv_ref, query_gain_ref, key_gain_ref, table_ref, wo_ref,
+    out_ref,
+    own_x, low_x, high_x, ctx_x, ws, wq, wk, wv, wo,
+    sums, plane_in, sums_z, z_in, final, mod, gain_row,
+    q_buf, k_buf, v_buf, ck_buf, cv_buf, lines, bias_buf, bound_buf, ctx_acc, mix,
+    local_sem, plane_send, plane_recv, z_send, z_recv, ctx_send, ctx_recv,
+    halo_send, halo_recv, tp_send, tp_recv,
+):
+    f32, bf16 = jnp.float32, jnp.bfloat16
+    me, mine = lax.axis_index("sp"), lax.axis_index("tp")
+    size = lax.axis_size("sp")
+    other = 1 - mine
+    mesh_ids = pl.DeviceIdType.MESH
+    tokens, width = own_x.shape
+    block = context_ref.shape[0]
+    share = width // 2
+    lane = wq.shape[1]
+    pairs = lane // LANES
+    rows_dev = tokens // GRID_W
+    reach = WIN_ROWS // 2
+    halo = reach * GRID_W
+    half_ctx = ctx_x.shape[0] // 2
+    cols = pl.ds(pl.multiple_of(mine * share, share), share)
+
+    def flip(mask):
+        index = me
+        bit = 1
+        while bit < size:
+            if mask & bit:
+                index = bit_flip(index, bit)
+            bit *= 2
+        return index
+
+    def remote(source, target, send, recv, where):
+        return pltpu.make_async_remote_copy(
+            src_ref=source, dst_ref=target, send_sem=send, recv_sem=recv,
+            device_id=where, device_id_type=mesh_ids,
+        )
+
+    plane = [1, 2, 3]
+    depth = [4 * k for k in sorted(range(1, size // 4), key=lambda k: (k.bit_count(), k))]
+
+    streams = {}
+    for place, (name, source, target) in enumerate(
+        (
+            ("shift", shift_ref, ws.at[0]),
+            ("scale", scale_ref, ws.at[1]),
+            ("gate", gate_ref, ws.at[2]),
+            ("keep", context_ref.at[:, cols],
+             ctx_x.at[pl.ds(pl.multiple_of(me * block, block), block), cols]),
+            ("own", latent_ref, own_x),
+            ("wk", wk_ref, wk),
+            ("wv", wv_ref, wv),
+            ("wq", wq_ref, wq),
+            ("wo", wo_ref, wo),
+        )
+    ):
+        streams[name] = pltpu.make_async_copy(source, target, local_sem.at[place])
+        streams[name].start()
+
+    barrier = pltpu.get_barrier_semaphore()
+    for mask in plane + depth:
+        pl.semaphore_signal(
+            barrier, inc=1, device_id={"sp": flip(mask)}, device_id_type=mesh_ids
+        )
+    pl.semaphore_signal(barrier, inc=1, device_id={"tp": other}, device_id_type=mesh_ids)
+    for away in (1, size - 1):
+        pl.semaphore_signal(
+            barrier, inc=1, device_id={"sp": (me + away) % size}, device_id_type=mesh_ids
+        )
+
+    def silu(ref):
+        v = ref[...].astype(f32)
+        return (v / (1.0 + jnp.exp(-v))).astype(bf16)
+
+    acts = jnp.concatenate([silu(cond_ref), silu(cond_ctx_ref)], axis=0)
+    part = share // 2
+    for place, name in enumerate(("shift", "scale")):
+        streams[name].wait()
+        raw = jnp.dot(acts, ws[place], preferred_element_type=f32)
+        sums[2 * place : 2 * place + 2, 0:part] = raw[:, :part]
+        sums[4 + 2 * place : 6 + 2 * place, 0:part] = raw[:, part:]
+    streams["gate"].wait()
+    raw = jnp.dot(acts, ws[2], preferred_element_type=f32)
+    piece = share // 8
+    for k in range(8):
+        sums[k : k + 1, part : part + piece] = raw[0:1, k * piece : (k + 1) * piece]
+
+    pl.semaphore_wait(barrier, len(plane) + len(depth) + 3)
+
+    first_stage = []
+    for place, mask in enumerate(plane):
+        copy = remote(
+            sums, plane_in.at[place], plane_send.at[place], plane_recv.at[place],
+            {"sp": flip(mask)},
+        )
+        copy.start()
+        first_stage.append(copy)
+
+    slots = {}
+
+    def ctx_copy(mask, toward):
+        slot = slots.setdefault((mask, toward), len(slots))
+        rows = pl.ds(pl.multiple_of(flip(mask) * block, block), block)
+        place = ctx_x.at[rows, cols]
+        return remote(
+            place, place, ctx_send.at[slot], ctx_recv.at[slot], {"sp": flip(toward)}
+        )
+
+    def ctx_arrival(mask, toward):
+        slot = slots[(mask, toward)]
+        rows = pl.ds(pl.multiple_of(flip(mask ^ toward) * block, block), block)
+        place = ctx_x.at[rows, cols]
+        remote(place, place, ctx_send.at[slot], ctx_recv.at[slot], {"sp": flip(toward)}).wait_recv()
+
+    streams["keep"].wait()
+    started = []
+
+    def ctx_start(mask, toward):
+        copy = ctx_copy(mask, toward)
+        copy.start()
+        started.append(copy)
+
+    ctx_start(0, 1)
+    ctx_start(0, 2)
+
+    up = remote(
+        latent_ref.at[pl.ds(tokens - halo, halo), cols], low_x.at[:, cols],
+        halo_send.at[0], halo_recv.at[0], {"sp": me + 1},
+    )
+    down = remote(
+        latent_ref.at[pl.ds(0, halo), cols], high_x.at[:, cols],
+        halo_send.at[1], halo_recv.at[1], {"sp": me - 1},
+    )
+    even = me % 2 == 0
+
+    @pl.when(even)
+    def _():
+        up.start()
+
+    @pl.when(jnp.logical_not(even))
+    def _():
+        down.start()
+
+    @pl.when(jnp.logical_and(even, me > 0))
+    def _():
+        down.start()
+
+    @pl.when(jnp.logical_and(jnp.logical_not(even), me < size - 1))
+    def _():
+        up.start()
+
+    for copy in first_stage:
+        copy.wait()
+    total = sums[...]
+    for place in range(len(plane)):
+        total = total + plane_in[place]
+    sums_z[...] = total
+    second_stage = []
+    for place, mask in enumerate(depth):
+        copy = remote(
+            sums_z, z_in.at[place], z_send.at[place], z_recv.at[place], {"sp": flip(mask)}
+        )
+        copy.start()
+        second_stage.append(copy)
+    for mask in depth:
+        ctx_start(0, mask)
+    ctx_arrival(0, 1)
+    for mask in depth:
+        ctx_start(1, mask)
+    ctx_start(1, 2)
+
+    norm_gain = norm_gain_ref[...].astype(f32)
+    for k in range(width // LANES):
+        gain_row[0:1, k * LANES : (k + 1) * LANES] = norm_gain[k : k + 1, :]
+    offsets = table_ref.shape[0]
+    span = table_ref.shape[2]
+    lines[...] = jnp.zeros_like(lines)
+    for k in range(offsets):
+        lines[k, :, 0:span] = table_ref[k]
+    for k in range(offsets):
+        lines[k] = lines[k] + pltpu.roll(lines[k + 1], GRID_W, 1)
+    for p in range(pairs):
+        filled = jnp.ones((v_buf.shape[0], LANES), bf16)
+        v_buf[:, (2 * p + 1) * LANES : (2 * p + 2) * LANES] = filled
+        cv_buf[:, (2 * p + 1) * LANES : (2 * p + 2) * LANES] = filled[: cv_buf.shape[0]]
+
+    base = me * rows_dev
+    query_col = lax.broadcasted_iota(jnp.int32, (GRID_W, LANES), 0)
+    lane_at = lax.broadcasted_iota(jnp.int32, (GRID_W, LANES), 1)
+    key_col = lane_at % GRID_W
+    window_first = jnp.clip(query_col - WIN_COLS // 2, 0, GRID_W - WIN_COLS)
+    inside = (key_col >= window_first) & (key_col < window_first + WIN_COLS)
+    per_tile = LANES // GRID_W
+    tiles_row = WIN_ROWS // per_tile
+
+    @pl.loop(0, pairs)
+    def _(pair):
+        for head in range(2):
+            for row in range(rows_dev):
+                first = jnp.clip(base + row - reach, 0, total_rows - WIN_ROWS)
+                offset = first - base - row + WIN_ROWS - 1
+                tiles = []
+                for tile in range(tiles_row):
+                    line = jnp.broadcast_to(
+                        lines[offset + tile * per_tile, pl.ds(pair * 2 + head, 1), :],
+                        (GRID_W, LANES),
+                    )
+                    moved = pltpu.roll(line, LANES - (WIN_COLS - 1), 1, stride=1, stride_axis=0)
+                    tiles.append(jnp.where(inside, moved, NEG))
+                top = tiles[0]
+                for tile in tiles[1:]:
+                    top = jnp.maximum(top, tile)
+                bound = jnp.maximum(jnp.max(top, axis=-1, keepdims=True), 0.0)
+                at = pl.ds(head * GRID_W, GRID_W)
+                for tile in range(tiles_row):
+                    bias_buf[pair, row, at, tile * LANES : (tile + 1) * LANES] = (
+                        tiles[tile] - bound
+                    ) * LOG2E
+                bound_buf[pair, pl.ds(head * tokens + row * GRID_W, GRID_W), :] = jnp.broadcast_to(
+                    bound * LOG2E, (GRID_W, LANES)
+                )
+
+    for copy in second_stage:
+        copy.wait()
+    total = sums_z[...]
+    for place in range(len(depth)):
+        total = total + z_in[place]
+    final[0] = total
+    swap = remote(final.at[0], final.at[1], tp_send.at[0], tp_recv.at[0], {"tp": other})
+    swap.start()
+    for mask in depth:
+        ctx_arrival(0, mask)
+        ctx_arrival(1, mask)
+        ctx_start(mask, 2)
+        ctx_start(mask ^ 1, 2)
+    swap.wait()
+    for side in range(2):
+        came = final[side]
+        at = pl.multiple_of((mine if side == 0 else other) * share, share)
+        mod[0:4, pl.ds(at, part)] = came[0:4, 0:part]
+        mod[0:4, pl.ds(at + part, part)] = came[4:8, 0:part]
+        for k in range(8):
+            mod[4:5, pl.ds(at + k * piece, piece)] = came[k : k + 1, part : part + piece]
+
+    norm = gain_row[...]
+    wide = 2 * LANES
+    half_r = lax.broadcasted_iota(jnp.int32, (wide, wide), 0) // HEAD_DIM
+    half_c = lax.broadcasted_iota(jnp.int32, (wide, wide), 1) // HEAD_DIM
+    ones = (half_r == half_c).astype(f32).astype(bf16)
+    heads = lane // HEAD_DIM
+    query_gain = jnp.concatenate(
+        [query_gain_ref[...].astype(f32) * (HEAD_DIM ** (-0.5) * LOG2E)] * heads, axis=1
+    )
+    key_gain = jnp.concatenate([key_gain_ref[...].astype(f32)] * heads, axis=1)
+
+    def normed(raw, gain):
+        square = (raw * raw).astype(bf16)
+        parts = [
+            jnp.dot(square[:, begin : begin + wide], ones, preferred_element_type=f32)
+            for begin in range(0, lane, wide)
+        ]
+        mean = jnp.concatenate(parts, axis=1) * (1.0 / HEAD_DIM)
+        return (raw * lax.rsqrt(mean + EPS) * gain).astype(bf16)
+
+    def hidden_of(x, shift, scale):
+        values = x.astype(f32)
+        inv = lax.rsqrt(jnp.mean(values * values, axis=-1, keepdims=True) + EPS)
+        return (values * inv * (norm * (1.0 + scale)) + shift).astype(bf16)
+
+    def keys_values(hidden, k_out, v_out, at):
+        count = hidden.shape[0]
+        raw = jnp.dot(hidden, wk[...], preferred_element_type=f32)
+        k_out[pl.ds(at, count), :] = normed(raw, key_gain)
+        raw = jnp.dot(hidden, wv[...], preferred_element_type=f32).astype(bf16)
+        for p in range(pairs):
+            v_out[pl.ds(at, count), 2 * p * LANES : (2 * p + 1) * LANES] = raw[
+                :, p * LANES : (p + 1) * LANES
+            ]
+
+    shift, shift_ctx = mod[0:1, :], mod[1:2, :]
+    scale, scale_ctx = mod[2:3, :], mod[3:4, :]
+    for name in ("own", "wk", "wv", "wq"):
+        streams[name].wait()
+    hidden = hidden_of(own_x[...], shift, scale)
+    keys_values(hidden, k_buf, v_buf, halo)
+    q_buf[...] = normed(jnp.dot(hidden, wq[...], preferred_element_type=f32), query_gain)
+
+    def spread(ref, rows, slot):
+        copy = remote(
+            ref.at[rows, cols], ref.at[rows, cols], tp_send.at[slot], tp_recv.at[slot],
+            {"tp": other},
+        )
+        copy.start()
+
+    def finish(ref, rows, slot):
+        theirs = pl.ds(pl.multiple_of(other * share, share), share)
+        copy = remote(
+            ref.at[rows, theirs], ref.at[rows, theirs], tp_send.at[slot], tp_recv.at[slot],
+            {"tp": other},
+        )
+        copy.wait_send()
+        copy.wait_recv()
+
+    every = pl.ds(0, halo)
+    for mask in [0, 1] + [m for d in depth for m in (d, d ^ 1)]:
+        ctx_arrival(mask, 2)
+    all_ctx = pl.ds(0, ctx_x.shape[0])
+    spread(ctx_x, all_ctx, 1)
+
+    @pl.when(me > 0)
+    def _():
+        up.wait_recv()
+        spread(low_x, every, 2)
+
+    finish(ctx_x, all_ctx, 1)
+
+    @pl.loop(0, 2)
+    def _(part_ctx):
+        at = pl.multiple_of(part_ctx * half_ctx, half_ctx)
+        hidden = hidden_of(ctx_x[pl.ds(at, half_ctx), :], shift_ctx, scale_ctx)
+        keys_values(hidden, ck_buf, cv_buf, at)
+
+    contract = (((1,), (1,)), ((), ()))
+
+    def two_heads(query):
+        zero = jnp.zeros_like(query)
+        left = lax.broadcasted_iota(jnp.int32, query.shape, 1) < HEAD_DIM
+        return jnp.concatenate(
+            [jnp.where(left, query, zero), jnp.where(left, zero, query)], axis=0
+        )
+
+    @pl.loop(0, pairs)
+    def _(pair):
+        at = pl.ds(pl.multiple_of(pair * LANES, LANES), LANES)
+        at2 = pl.ds(pl.multiple_of(pair * 2 * LANES, 2 * LANES), 2 * LANES)
+        score = lax.dot_general(
+            two_heads(q_buf[:, at]), ck_buf[:, at], contract, preferred_element_type=f32
+        )
+        bound = bound_buf[pair]
+        shown = jnp.concatenate([bound] * (score.shape[1] // LANES), axis=1)
+        weight = jnp.exp2(score - shown).astype(bf16)
+        ctx_acc[pair] = jnp.dot(weight, cv_buf[:, at2], preferred_element_type=f32)
+
+    @pl.when(me > 0)
+    def _():
+        finish(low_x, every, 2)
+
+    keys_values(hidden_of(low_x[...], shift, scale), k_buf, v_buf, 0)
+
+    @pl.when(me < size - 1)
+    def _():
+        down.wait_recv()
+        spread(high_x, every, 3)
+        finish(high_x, every, 3)
+
+    keys_values(hidden_of(high_x[...], shift, scale), k_buf, v_buf, halo + tokens)
+
+    def mix_copy(pair):
+        at = pl.ds(pl.multiple_of(pair * LANES, LANES), LANES)
+        return remote(
+            mix.at[0, :, at], mix.at[1, :, at], tp_send.at[4 + pair], tp_recv.at[4 + pair],
+            {"tp": other},
+        )
+
+    first_head = lane_at < HEAD_DIM
+
+    @pl.loop(0, pairs)
+    def _(pair):
+        at = pl.ds(pl.multiple_of(pair * LANES, LANES), LANES)
+        at2 = pl.ds(pl.multiple_of(pair * 2 * LANES, 2 * LANES), 2 * LANES)
+        for row in range(rows_dev):
+            first = jnp.clip(base + row - reach, 0, total_rows - WIN_ROWS)
+            begin = pl.multiple_of((first - base + reach) * GRID_W, GRID_W)
+            mine_rows = slice(row * GRID_W, (row + 1) * GRID_W)
+            theirs = slice(tokens + row * GRID_W, tokens + (row + 1) * GRID_W)
+            band = pl.ds(begin, WIN_ROWS * GRID_W)
+            score = lax.dot_general(
+                two_heads(q_buf[mine_rows, at]), k_buf[band, at], contract,
+                preferred_element_type=f32,
+            )
+            weight = jnp.exp2(score + bias_buf[pair, row]).astype(bf16)
+            acc = jnp.dot(weight, v_buf[band, at2], preferred_element_type=f32)
+            left = acc[:GRID_W] + ctx_acc[pair, mine_rows, :]
+            right = acc[GRID_W:] + ctx_acc[pair, theirs, :]
+            mix[0, mine_rows, at] = jnp.where(
+                first_head,
+                left[:, :LANES] / left[:, LANES:],
+                right[:, :LANES] / right[:, LANES:],
+            ).astype(bf16)
+        mix_copy(pair).start()
+
+    streams["wo"].wait()
+    out = jnp.dot(
+        mix[0], wo[pl.ds(pl.multiple_of(mine * lane, lane), lane), :], preferred_element_type=f32
+    )
+    for pair in range(pairs):
+        mix_copy(pair).wait()
+    out = out + jnp.dot(
+        mix[1], wo[pl.ds(pl.multiple_of(other * lane, lane), lane), :], preferred_element_type=f32
+    )
+    out_ref[...] = (own_x[:, cols].astype(f32) + mod[4:5, cols] * out).astype(bf16)
+
+    for copy in started:
+        copy.wait_send()
+
+    @pl.when(me < size - 1)
+    def _():
+        up.wait_send()
+
+    @pl.when(me > 0)
+    def _():
+        down.wait_send()
+
+
+def fused_body(
+    latent, context, cond, cond_ctx, shift_weight, scale_weight, gate_weight, norm_gain,
+    query_weight, key_weight, value_weight, query_gain, key_gain, offset_bias, out_weight,
+):
+    size = lax.axis_size("sp")
+    total_rows = (latent.shape[0] // GRID_W) * size
+    tokens, width = latent.shape
+    share, lane = shift_weight.shape[1], query_weight.shape[1]
+    halo = WIN_ROWS // 2 * GRID_W
+    kv_rows = tokens + 2 * halo
+    ctx_rows = context.shape[0] * size
+    pairs = lane // LANES
+    packed = share // 2 + share // 8
+    depth = size // 4 - 1
+    copies = 4 + 4 * depth
+    bf16, f32 = jnp.bfloat16, jnp.float32
+    vmem = pl.BlockSpec(memory_space=pltpu.VMEM)
+    hbm = pl.BlockSpec(memory_space=pl.ANY)
+    dma = pltpu.SemaphoreType.DMA
+    return pl.pallas_call(
+        functools.partial(fused_kernel, total_rows),
+        out_shape=jax.ShapeDtypeStruct((tokens, share), latent.dtype),
+        in_specs=[hbm] * 2 + [vmem] * 2 + [hbm] * 3 + [vmem] + [hbm] * 3 + [vmem] * 3 + [hbm],
+        out_specs=vmem,
+        scratch_shapes=[
+            pltpu.VMEM((tokens, width), bf16),
+            pltpu.VMEM((halo, width), bf16),
+            pltpu.VMEM((halo, width), bf16),
+            pltpu.VMEM((ctx_rows, width), bf16),
+            pltpu.VMEM((3,) + shift_weight.shape, bf16),
+            pltpu.VMEM(query_weight.shape, bf16),
+            pltpu.VMEM(key_weight.shape, bf16),
+            pltpu.VMEM(value_weight.shape, bf16),
+            pltpu.VMEM(out_weight.shape, bf16),
+            pltpu.VMEM((8, packed), f32),
+            pltpu.VMEM((3, 8, packed), f32),
+            pltpu.VMEM((8, packed), f32),
+            pltpu.VMEM((depth, 8, packed), f32),
+            pltpu.VMEM((2, 8, packed), f32),
+            pltpu.VMEM((8, width), f32),
+            pltpu.VMEM((1, width), f32),
+            pltpu.VMEM((tokens, lane), bf16),
+            pltpu.VMEM((kv_rows, lane), bf16),
+            pltpu.VMEM((kv_rows, 2 * lane), bf16),
+            pltpu.VMEM((ctx_rows, lane), bf16),
+            pltpu.VMEM((ctx_rows, 2 * lane), bf16),
+            pltpu.VMEM((2 * WIN_ROWS, offset_bias.shape[0], LANES), f32),
+            pltpu.VMEM((pairs, tokens // GRID_W, LANES, WIN_ROWS * GRID_W), f32),
+            pltpu.VMEM((pairs, 2 * tokens, LANES), f32),
+            pltpu.VMEM((pairs, 2 * tokens, 2 * LANES), f32),
+            pltpu.VMEM((2, tokens, lane), bf16),
+            dma((9,)),
+            dma((3,)), dma((3,)),
+            dma((depth,)), dma((depth,)),
+            dma((copies,)), dma((copies,)),
+            dma((2,)), dma((2,)),
+            dma((4 + pairs,)), dma((4 + pairs,)),
+        ],
+        compiler_params=pltpu.CompilerParams(collective_id=0, has_side_effects=True),
+        name="fused",
+    )(
+        latent, context, cond[None, :], cond_ctx[None, :],
+        shift_weight, scale_weight, gate_weight,
+        norm_gain.reshape(width // LANES, LANES),
+        query_weight, key_weight, value_weight,
+        query_gain[None, :], key_gain[None, :],
+        jnp.transpose(offset_bias, (1, 0, 2)),
+        out_weight,
+    )
+
+
 def choose(latent, context, *rest):
     rows_dev = latent.shape[0] // GRID_W
     lane = rest[6].shape[1]
     size = lax.axis_size("sp")
     fits = size >= 4 and size & (size - 1) == 0 and context.shape[0] % 8 == 0
-    if fits and lane % LANES == 0 and rows_dev >= WIN_ROWS // 2 and 2 * GRID_W == LANES:
+    aligned = lane % LANES == 0 and 2 * GRID_W == LANES
+    if fits and aligned and lax.axis_size("tp") == 2 and rows_dev == WIN_ROWS // 2:
+        return fused_body(latent, context, *rest)
+    if fits and aligned and rows_dev >= WIN_ROWS // 2:
         return fast_body(latent, context, *rest)
     return body(latent, context, *rest)
 

time: 77.4 us -> 61 us (0.79)
  Pallas kernels: 67.5 us -> 58.9 us
  blocking collectives: 3.84 us -> 0 us
  matrix products: 2.56 us -> 0 us
  local copies, waits for them, and re-layouts: 3.01 us -> 1.87 us
    pallas_call x2 -> x1, Pallas kernels: 67.5 us -> 58.9 us  [fused_body(): pl.pallas_call(functools.partial(fused_kernel, total_rows), out_shape=jax...]
    all_gather x1 -> x0, blocking collectives: 3.84 us -> none  [fast_body(): lax.all_gather(mixed, 'tp', axis=1, tiled=True)]
    dot_general x1 -> x0, matrix products: 2.56 us -> none  [fast_body(): jnp.dot(lax.all_gather(mixed, 'tp', axis=1, tiled=True), out_weight, pref...]
    unnamed x6 -> x1, local copies, waits for them, and re-layouts: 0.01 us -> 1.87 us
    slice x2 -> x0, local copies, waits for them, and re-layouts: 1.76 us -> none  [the longest x1 0.91 us: bias_lines(): lines = jnp.concatenate([wide[:, :-1], wide[:, 1:]], axis=2)]
where the time goes in v1:
time: 61 us; the launch traced here: 60.8 us
  Pallas kernels  58.9 us (97%)
  local copies, waits for them, and re-layouts  1.87 us (3%)
    pallas_call x1, Pallas kernels, fused_body(): pl.pallas_call(functools.partial(fused_kernel, total_rows), out_shape=jax...  58.9 us
    unnamed x1, local copies, waits for them, and re-layouts  1.87 us

profile of v1, /device:TPU:3, one launch (start us, length us, event | category | flops | bytes accessed | tf_op | source)
XLA Modules:
  0.0 60.8 jit_solution(12871725338948851836)
XLA Ops:
  0.0 58.9 %fused.1 = bf16[256,1024]{1,0:T(8,128)(2,1)} custom-call(bf16[256,2048]{1,0:T(8,128)(2,1)} %latent_ref.1, bf16[32,2048]{1,0:T(8,128)(2,1)} %context_ref.1, bf16[1,128]{1,0:T(2,128)(2,1)} %bitcast.8, bf16[1,128]{1,0:T(2,128)(2,1)} %bitcast.9, bf16[128,1024]{1,0:T(8,128)(2,1)} %shift_ref.1, bf16[128,1024]{1,0:T(8,128)(2,1)} %scale_ref.1, ...), custom_call_target="tpu_custom_call" | custom-call | tf_op jit(solution)/shard_map/fused/pallas_call | solution.py:1084
  59.0 1.9 %copy.17 = bf16[256,1024]{1,0:T(8,128)(2,1)} copy(bf16[256,1024]{1,0:T(8,128)(2,1)} %fused.1) | data formatting | bytes 1048576

commit v2 on v1

--- a/solution.py
+++ b/solution.py
@@ -646,14 +646,15 @@
 
 def fused_kernel(
     total_rows,
-    latent_ref, context_ref, cond_ref, cond_ctx_ref, shift_ref, scale_ref, gate_ref,
-    norm_gain_ref, wq_ref, wk_ref, wv_ref, query_gain_ref, key_gain_ref, table_ref, wo_ref,
+    latent_ref, context_ref, cond_hbm, cond_ctx_hbm, shift_ref, scale_ref, gate_ref,
+    norm_gain_hbm, wq_ref, wk_ref, wv_ref, query_gain_hbm, key_gain_hbm, table_hbm, wo_ref,
     out_ref,
-    own_x, low_x, high_x, ctx_x, ws, wq, wk, wv, wo,
+    cond_ref, cond_ctx_ref, norm_gain_ref, query_gain_ref, key_gain_ref, table_ref,
+    own_x, halo_x, ctx_x, ws, wq, wk, wv, wo,
     sums, plane_in, sums_z, z_in, final, mod, gain_row,
-    q_buf, k_buf, v_buf, ck_buf, cv_buf, lines, bias_buf, bound_buf, ctx_acc, mix,
+    q_buf, k_buf, v_buf, ck_buf, cv_buf, lines, bias_buf, bound_buf, near, mix,
     local_sem, plane_send, plane_recv, z_send, z_recv, ctx_send, ctx_recv,
-    halo_send, halo_recv, tp_send, tp_recv,
+    halo_send, halo_recv, relay_send, relay_recv, tp_send, tp_recv,
 ):
     f32, bf16 = jnp.float32, jnp.bfloat16
     me, mine = lax.axis_index("sp"), lax.axis_index("tp")
@@ -692,11 +693,17 @@
     streams = {}
     for place, (name, source, target) in enumerate(
         (
+            ("cond", cond_hbm, cond_ref),
+            ("cond_ctx", cond_ctx_hbm, cond_ctx_ref),
             ("shift", shift_ref, ws.at[0]),
             ("scale", scale_ref, ws.at[1]),
             ("gate", gate_ref, ws.at[2]),
             ("keep", context_ref.at[:, cols],
              ctx_x.at[pl.ds(pl.multiple_of(me * block, block), block), cols]),
+            ("table", table_hbm, table_ref),
+            ("norm_gain", norm_gain_hbm, norm_gain_ref),
+            ("query_gain", query_gain_hbm, query_gain_ref),
+            ("key_gain", key_gain_hbm, key_gain_ref),
             ("own", latent_ref, own_x),
             ("wk", wk_ref, wk),
             ("wv", wv_ref, wv),
@@ -705,7 +712,17 @@
         )
     ):
         streams[name] = pltpu.make_async_copy(source, target, local_sem.at[place])
-        streams[name].start()
+
+    def fetch(*names):
+        for name in names:
+            streams[name].start()
+
+    def arrived(*names):
+        for name in names:
+            streams[name].wait()
+
+    fetch("cond", "cond_ctx", "shift", "scale", "gate", "keep", "table")
+    fetch("norm_gain", "query_gain", "key_gain")
 
     barrier = pltpu.get_barrier_semaphore()
     for mask in plane + depth:
@@ -713,112 +730,34 @@
             barrier, inc=1, device_id={"sp": flip(mask)}, device_id_type=mesh_ids
         )
     pl.semaphore_signal(barrier, inc=1, device_id={"tp": other}, device_id_type=mesh_ids)
-    for away in (1, size - 1):
-        pl.semaphore_signal(
-            barrier, inc=1, device_id={"sp": (me + away) % size}, device_id_type=mesh_ids
-        )
+    parity = me % 2
+    ahead = me + 2 - 4 * parity
+    behind = me - 2 + 4 * parity
+    pl.semaphore_signal(
+        barrier, inc=1, device_id={"sp": (ahead + size) % size}, device_id_type=mesh_ids
+    )
+    pl.semaphore_signal(
+        barrier, inc=1, device_id={"sp": (behind + size) % size}, device_id_type=mesh_ids
+    )
 
     def silu(ref):
         v = ref[...].astype(f32)
         return (v / (1.0 + jnp.exp(-v))).astype(bf16)
 
+    arrived("cond", "cond_ctx", "shift", "scale", "gate")
+    fetch("own", "wk", "wv", "wq", "wo")
     acts = jnp.concatenate([silu(cond_ref), silu(cond_ctx_ref)], axis=0)
     part = share // 2
-    for place, name in enumerate(("shift", "scale")):
-        streams[name].wait()
+    for place in range(2):
         raw = jnp.dot(acts, ws[place], preferred_element_type=f32)
         sums[2 * place : 2 * place + 2, 0:part] = raw[:, :part]
         sums[4 + 2 * place : 6 + 2 * place, 0:part] = raw[:, part:]
-    streams["gate"].wait()
     raw = jnp.dot(acts, ws[2], preferred_element_type=f32)
     piece = share // 8
     for k in range(8):
         sums[k : k + 1, part : part + piece] = raw[0:1, k * piece : (k + 1) * piece]
 
-    pl.semaphore_wait(barrier, len(plane) + len(depth) + 3)
-
-    first_stage = []
-    for place, mask in enumerate(plane):
-        copy = remote(
-            sums, plane_in.at[place], plane_send.at[place], plane_recv.at[place],
-            {"sp": flip(mask)},
-        )
-        copy.start()
-        first_stage.append(copy)
-
-    slots = {}
-
-    def ctx_copy(mask, toward):
-        slot = slots.setdefault((mask, toward), len(slots))
-        rows = pl.ds(pl.multiple_of(flip(mask) * block, block), block)
-        place = ctx_x.at[rows, cols]
-        return remote(
-            place, place, ctx_send.at[slot], ctx_recv.at[slot], {"sp": flip(toward)}
-        )
-
-    def ctx_arrival(mask, toward):
-        slot = slots[(mask, toward)]
-        rows = pl.ds(pl.multiple_of(flip(mask ^ toward) * block, block), block)
-        place = ctx_x.at[rows, cols]
-        remote(place, place, ctx_send.at[slot], ctx_recv.at[slot], {"sp": flip(toward)}).wait_recv()
-
-    streams["keep"].wait()
-    started = []
-
-    def ctx_start(mask, toward):
-        copy = ctx_copy(mask, toward)
-        copy.start()
-        started.append(copy)
-
-    ctx_start(0, 1)
-    ctx_start(0, 2)
-
-    up = remote(
-        latent_ref.at[pl.ds(tokens - halo, halo), cols], low_x.at[:, cols],
-        halo_send.at[0], halo_recv.at[0], {"sp": me + 1},
-    )
-    down = remote(
-        latent_ref.at[pl.ds(0, halo), cols], high_x.at[:, cols],
-        halo_send.at[1], halo_recv.at[1], {"sp": me - 1},
-    )
-    even = me % 2 == 0
-
-    @pl.when(even)
-    def _():
-        up.start()
-
-    @pl.when(jnp.logical_not(even))
-    def _():
-        down.start()
-
-    @pl.when(jnp.logical_and(even, me > 0))
-    def _():
-        down.start()
-
-    @pl.when(jnp.logical_and(jnp.logical_not(even), me < size - 1))
-    def _():
-        up.start()
-
-    for copy in first_stage:
-        copy.wait()
-    total = sums[...]
-    for place in range(len(plane)):
-        total = total + plane_in[place]
-    sums_z[...] = total
-    second_stage = []
-    for place, mask in enumerate(depth):
-        copy = remote(
-            sums_z, z_in.at[place], z_send.at[place], z_recv.at[place], {"sp": flip(mask)}
-        )
-        copy.start()
-        second_stage.append(copy)
-    for mask in depth:
-        ctx_start(0, mask)
-    ctx_arrival(0, 1)
-    for mask in depth:
-        ctx_start(1, mask)
-    ctx_start(1, 2)
-
+    arrived("keep", "table", "norm_gain", "query_gain", "key_gain")
     norm_gain = norm_gain_ref[...].astype(f32)
     for k in range(width // LANES):
         gain_row[0:1, k * LANES : (k + 1) * LANES] = norm_gain[k : k + 1, :]
@@ -843,8 +782,7 @@
     per_tile = LANES // GRID_W
     tiles_row = WIN_ROWS // per_tile
 
-    @pl.loop(0, pairs)
-    def _(pair):
+    def bias_of(pair):
         for head in range(2):
             for row in range(rows_dev):
                 first = jnp.clip(base + row - reach, 0, total_rows - WIN_ROWS)
@@ -870,6 +808,128 @@
                     bound * LOG2E, (GRID_W, LANES)
                 )
 
+    quarter = pairs // 4
+    pl.loop(0, quarter)(bias_of)
+    pl.semaphore_wait(barrier, len(plane) + len(depth) + 3)
+
+    first_stage = []
+    for place, mask in enumerate(plane):
+        copy = remote(
+            sums, plane_in.at[place], plane_send.at[place], plane_recv.at[place],
+            {"sp": flip(mask)},
+        )
+        copy.start()
+        first_stage.append(copy)
+
+    slots = {}
+
+    def ctx_copy(mask, toward):
+        slot = slots.setdefault((mask, toward), len(slots))
+        rows = pl.ds(pl.multiple_of(flip(mask) * block, block), block)
+        place = ctx_x.at[rows, cols]
+        return remote(
+            place, place, ctx_send.at[slot], ctx_recv.at[slot], {"sp": flip(toward)}
+        )
+
+    def ctx_arrival(mask, toward):
+        slot = slots[(mask, toward)]
+        rows = pl.ds(pl.multiple_of(flip(mask ^ toward) * block, block), block)
+        place = ctx_x.at[rows, cols]
+        remote(place, place, ctx_send.at[slot], ctx_recv.at[slot], {"sp": flip(toward)}).wait_recv()
+
+    started = []
+
+    def ctx_start(mask, toward):
+        copy = ctx_copy(mask, toward)
+        copy.start()
+        started.append(copy)
+
+    ctx_start(0, 1)
+    ctx_start(0, 2)
+
+    chunks = reach
+    step = halo // chunks
+
+    def partner_copy(k):
+        rows = pl.ds(k * step, step)
+        return remote(
+            latent_ref.at[rows, cols], halo_x.at[parity, rows, cols],
+            halo_send.at[k], halo_recv.at[k], {"sp": flip(1)},
+        )
+
+    def relay_copy(k):
+        rows = pl.ds(k * step, step)
+        return remote(
+            halo_x.at[1 - parity, rows, cols], halo_x.at[parity, rows, cols],
+            relay_send.at[k], relay_recv.at[k], {"sp": ahead},
+        )
+
+    has_ahead = jnp.logical_and(ahead >= 0, ahead < size)
+    has_behind = jnp.logical_and(behind >= 0, behind < size)
+
+    def spread(ref, rows, slot):
+        remote(
+            ref.at[rows, cols], ref.at[rows, cols], tp_send.at[slot], tp_recv.at[slot],
+            {"tp": other},
+        ).start()
+
+    def finish(ref, rows, slot):
+        theirs = pl.ds(pl.multiple_of(other * share, share), share)
+        copy = remote(
+            ref.at[rows, theirs], ref.at[rows, theirs], tp_send.at[slot], tp_recv.at[slot],
+            {"tp": other},
+        )
+        copy.wait_send()
+        copy.wait_recv()
+
+    def relay(k):
+        partner_copy(k).wait_recv()
+
+        @pl.when(has_ahead)
+        def _():
+            relay_copy(k).start()
+
+        spread(halo_x.at[1 - parity], pl.ds(k * step, step), 1 + k)
+
+    def plane_rows(mask):
+        return pl.ds(pl.multiple_of(flip(mask) // 4 * 4 * block, 4 * block), 4 * block)
+
+    def plane_slot(mask):
+        return 1 + 2 * chunks + mask // 4
+
+    near_masks = [mask for mask in depth if mask < size // 2]
+    far_masks = [mask for mask in depth if mask >= size // 2][::-1]
+    via_x, via_y = far_masks[: len(far_masks) // 2], far_masks[len(far_masks) // 2 :]
+    partner_copy(0).start()
+    for mask in near_masks:
+        ctx_start(0, mask)
+
+    pl.loop(quarter, 2 * quarter)(bias_of)
+    for copy in first_stage:
+        copy.wait()
+    total = sums[...]
+    for place in range(len(plane)):
+        total = total + plane_in[place]
+    sums_z[...] = total
+    second_stage = []
+    for place, mask in enumerate(depth):
+        copy = remote(
+            sums_z, z_in.at[place], z_send.at[place], z_recv.at[place], {"sp": flip(mask)}
+        )
+        copy.start()
+        second_stage.append(copy)
+    ctx_arrival(0, 1)
+    ctx_start(1, 2)
+    for mask in near_masks:
+        ctx_arrival(0, mask)
+        ctx_start(mask, 1)
+        ctx_start(mask, 2)
+    for k in range(1, chunks):
+        partner_copy(k).start()
+
+    pl.loop(2 * quarter, 3 * quarter)(bias_of)
+    relay(0)
+    pl.loop(3 * quarter, pairs)(bias_of)
     for copy in second_stage:
         copy.wait()
     total = sums_z[...]
@@ -878,10 +938,13 @@
     final[0] = total
     swap = remote(final.at[0], final.at[1], tp_send.at[0], tp_recv.at[0], {"tp": other})
     swap.start()
-    for mask in depth:
-        ctx_arrival(0, mask)
-        ctx_arrival(1, mask)
-        ctx_start(mask, 2)
+    for mask in far_masks:
+        ctx_start(0, mask)
+    ctx_arrival(0, 2)
+    ctx_arrival(1, 2)
+    spread(ctx_x, plane_rows(0), plane_slot(0))
+    for mask in near_masks:
+        ctx_arrival(mask, 1)
         ctx_start(mask ^ 1, 2)
     swap.wait()
     for side in range(2):
@@ -929,46 +992,39 @@
 
     shift, shift_ctx = mod[0:1, :], mod[1:2, :]
     scale, scale_ctx = mod[2:3, :], mod[3:4, :]
-    for name in ("own", "wk", "wv", "wq"):
-        streams[name].wait()
+    arrived("own", "wk", "wv", "wq")
     hidden = hidden_of(own_x[...], shift, scale)
     keys_values(hidden, k_buf, v_buf, halo)
+    relay(1)
     q_buf[...] = normed(jnp.dot(hidden, wq[...], preferred_element_type=f32), query_gain)
 
-    def spread(ref, rows, slot):
-        copy = remote(
-            ref.at[rows, cols], ref.at[rows, cols], tp_send.at[slot], tp_recv.at[slot],
-            {"tp": other},
-        )
-        copy.start()
-
-    def finish(ref, rows, slot):
-        theirs = pl.ds(pl.multiple_of(other * share, share), share)
-        copy = remote(
-            ref.at[rows, theirs], ref.at[rows, theirs], tp_send.at[slot], tp_recv.at[slot],
-            {"tp": other},
-        )
-        copy.wait_send()
-        copy.wait_recv()
-
-    every = pl.ds(0, halo)
-    for mask in [0, 1] + [m for d in depth for m in (d, d ^ 1)]:
+    for mask in near_masks:
         ctx_arrival(mask, 2)
-    all_ctx = pl.ds(0, ctx_x.shape[0])
-    spread(ctx_x, all_ctx, 1)
-
-    @pl.when(me > 0)
-    def _():
-        up.wait_recv()
-        spread(low_x, every, 2)
-
-    finish(ctx_x, all_ctx, 1)
-
-    @pl.loop(0, 2)
-    def _(part_ctx):
-        at = pl.multiple_of(part_ctx * half_ctx, half_ctx)
+        ctx_arrival(mask ^ 1, 2)
+        spread(ctx_x, plane_rows(mask), plane_slot(mask))
+    for mask in [0] + near_masks:
+        finish(ctx_x, plane_rows(mask), plane_slot(mask))
+
+    def between(far):
+        if far:
+            return
+        relay(2)
+        for mask in far_masks:
+            ctx_arrival(0, mask)
+            ctx_start(mask, 1)
+
+    def ctx_half(far):
+        top = size // 2
+        index = me // top
+        if far:
+            index = 1 - index
+        at = pl.multiple_of(index * half_ctx, half_ctx)
         hidden = hidden_of(ctx_x[pl.ds(at, half_ctx), :], shift_ctx, scale_ctx)
+        between(far)
         keys_values(hidden, ck_buf, cv_buf, at)
+        return pl.ds(at, half_ctx)
+
+    near_rows = ctx_half(False)
 
     contract = (((1,), (1,)), ((), ()))
 
@@ -979,50 +1035,62 @@
             [jnp.where(left, query, zero), jnp.where(left, zero, query)], axis=0
         )
 
-    @pl.loop(0, pairs)
-    def _(pair):
+    def from_ctx(pair, rows):
         at = pl.ds(pl.multiple_of(pair * LANES, LANES), LANES)
         at2 = pl.ds(pl.multiple_of(pair * 2 * LANES, 2 * LANES), 2 * LANES)
         score = lax.dot_general(
-            two_heads(q_buf[:, at]), ck_buf[:, at], contract, preferred_element_type=f32
-        )
-        bound = bound_buf[pair]
-        shown = jnp.concatenate([bound] * (score.shape[1] // LANES), axis=1)
+            two_heads(q_buf[:, at]), ck_buf[rows, at], contract, preferred_element_type=f32
+        )
+        shown = jnp.concatenate([bound_buf[pair]] * (half_ctx // LANES), axis=1)
         weight = jnp.exp2(score - shown).astype(bf16)
-        ctx_acc[pair] = jnp.dot(weight, cv_buf[:, at2], preferred_element_type=f32)
-
-    @pl.when(me > 0)
-    def _():
-        finish(low_x, every, 2)
-
-    keys_values(hidden_of(low_x[...], shift, scale), k_buf, v_buf, 0)
-
-    @pl.when(me < size - 1)
-    def _():
-        down.wait_recv()
-        spread(high_x, every, 3)
-        finish(high_x, every, 3)
-
-    keys_values(hidden_of(high_x[...], shift, scale), k_buf, v_buf, halo + tokens)
-
-    def mix_copy(pair):
-        at = pl.ds(pl.multiple_of(pair * LANES, LANES), LANES)
-        return remote(
-            mix.at[0, :, at], mix.at[1, :, at], tp_send.at[4 + pair], tp_recv.at[4 + pair],
-            {"tp": other},
-        )
-
-    first_head = lane_at < HEAD_DIM
+        return jnp.dot(weight, cv_buf[rows, at2], preferred_element_type=f32)
 
     @pl.loop(0, pairs)
     def _(pair):
+        near[pair] = from_ctx(pair, near_rows)
+
+    for k in range(3, chunks):
+        relay(k)
+    for mask in far_masks:
+        ctx_start(mask, 2)
+    for k in range(chunks):
+        finish(halo_x.at[1 - parity], pl.ds(k * step, step), 1 + k)
+    stride = halo + tokens
+    keys_values(
+        hidden_of(halo_x[1 - parity], shift, scale),
+        k_buf, v_buf, pl.multiple_of((1 - parity) * stride, stride),
+    )
+    for mask in via_y:
+        ctx_arrival(mask, 1)
+        ctx_start(mask ^ 1, 2)
+
+    @pl.when(has_behind)
+    def _():
+        for k in range(chunks):
+            relay_copy(k).wait_recv()
+            spread(halo_x.at[parity], pl.ds(k * step, step), 1 + chunks + k)
+
+    for mask in via_x:
+        ctx_arrival(mask, 2)
+        ctx_start(mask ^ 2, 1)
+
+    @pl.when(has_behind)
+    def _():
+        for k in range(chunks):
+            finish(halo_x.at[parity], pl.ds(k * step, step), 1 + chunks + k)
+
+    keys_values(
+        hidden_of(halo_x[parity], shift, scale),
+        k_buf, v_buf, pl.multiple_of(parity * stride, stride),
+    )
+
+    def from_window(pair):
         at = pl.ds(pl.multiple_of(pair * LANES, LANES), LANES)
         at2 = pl.ds(pl.multiple_of(pair * 2 * LANES, 2 * LANES), 2 * LANES)
         for row in range(rows_dev):
             first = jnp.clip(base + row - reach, 0, total_rows - WIN_ROWS)
             begin = pl.multiple_of((first - base + reach) * GRID_W, GRID_W)
             mine_rows = slice(row * GRID_W, (row + 1) * GRID_W)
-            theirs = slice(tokens + row * GRID_W, tokens + (row + 1) * GRID_W)
             band = pl.ds(begin, WIN_ROWS * GRID_W)
             score = lax.dot_general(
                 two_heads(q_buf[mine_rows, at]), k_buf[band, at], contract,
@@ -1030,16 +1098,43 @@
             )
             weight = jnp.exp2(score + bias_buf[pair, row]).astype(bf16)
             acc = jnp.dot(weight, v_buf[band, at2], preferred_element_type=f32)
-            left = acc[:GRID_W] + ctx_acc[pair, mine_rows, :]
-            right = acc[GRID_W:] + ctx_acc[pair, theirs, :]
-            mix[0, mine_rows, at] = jnp.where(
-                first_head,
-                left[:, :LANES] / left[:, LANES:],
-                right[:, :LANES] / right[:, LANES:],
-            ).astype(bf16)
+            near[pair, mine_rows, :] += acc[:GRID_W]
+            near[pair, tokens + row * GRID_W : tokens + (row + 1) * GRID_W, :] += acc[GRID_W:]
+
+    pl.loop(0, pairs // 2)(from_window)
+    for mask in via_x:
+        ctx_arrival(mask, 1)
+        ctx_arrival(mask ^ 2, 1)
+    for mask in via_y:
+        ctx_arrival(mask, 2)
+        ctx_arrival(mask ^ 1, 2)
+    for mask in far_masks:
+        spread(ctx_x, plane_rows(mask), plane_slot(mask))
+    pl.loop(pairs // 2, pairs)(from_window)
+
+    for mask in far_masks:
+        finish(ctx_x, plane_rows(mask), plane_slot(mask))
+    far_rows = ctx_half(True)
+
+    mix_slot = plane_slot(0) + size // 4
+
+    def mix_copy(pair):
+        at = pl.ds(pl.multiple_of(pair * LANES, LANES), LANES)
+        return remote(
+            mix.at[0, :, at], mix.at[1, :, at],
+            tp_send.at[mix_slot + pair], tp_recv.at[mix_slot + pair], {"tp": other},
+        )
+
+    @pl.loop(0, pairs)
+    def _(pair):
+        at = pl.ds(pl.multiple_of(pair * LANES, LANES), LANES)
+        acc = near[pair] + from_ctx(pair, far_rows)
+        mixed = acc[:, :LANES] / acc[:, LANES:]
+        left = lax.broadcasted_iota(jnp.int32, (tokens, LANES), 1) < HEAD_DIM
+        mix[0, :, at] = jnp.where(left, mixed[:tokens], mixed[tokens:]).astype(bf16)
         mix_copy(pair).start()
 
-    streams["wo"].wait()
+    arrived("wo")
     out = jnp.dot(
         mix[0], wo[pl.ds(pl.multiple_of(mine * lane, lane), lane), :], preferred_element_type=f32
     )
@@ -1053,13 +1148,13 @@
     for copy in started:
         copy.wait_send()
 
-    @pl.when(me < size - 1)
+    for k in range(chunks):
+        partner_copy(k).wait_send()
+
+    @pl.when(has_ahead)
     def _():
-        up.wait_send()
-
-    @pl.when(me > 0)
-    def _():
-        down.wait_send()
+        for k in range(chunks):
+            relay_copy(k).wait_send()
 
 
 def fused_body(
@@ -1070,26 +1165,33 @@
     total_rows = (latent.shape[0] // GRID_W) * size
     tokens, width = latent.shape
     share, lane = shift_weight.shape[1], query_weight.shape[1]
-    halo = WIN_ROWS // 2 * GRID_W
+    reach = WIN_ROWS // 2
+    halo = reach * GRID_W
     kv_rows = tokens + 2 * halo
     ctx_rows = context.shape[0] * size
     pairs = lane // LANES
     packed = share // 2 + share // 8
     depth = size // 4 - 1
     copies = 4 + 4 * depth
+    swaps = 1 + 2 * reach + size // 4 + pairs
     bf16, f32 = jnp.bfloat16, jnp.float32
     vmem = pl.BlockSpec(memory_space=pltpu.VMEM)
-    hbm = pl.BlockSpec(memory_space=pl.ANY)
+    hbm = pl.BlockSpec(memory_space=pltpu.HBM)
     dma = pltpu.SemaphoreType.DMA
     return pl.pallas_call(
         functools.partial(fused_kernel, total_rows),
-        out_shape=jax.ShapeDtypeStruct((tokens, share), latent.dtype),
-        in_specs=[hbm] * 2 + [vmem] * 2 + [hbm] * 3 + [vmem] + [hbm] * 3 + [vmem] * 3 + [hbm],
+        out_shape=pltpu.VMEM((tokens, share), latent.dtype),
+        in_specs=[hbm] * 15,
         out_specs=vmem,
         scratch_shapes=[
+            pltpu.VMEM((1,) + cond.shape, bf16),
+            pltpu.VMEM((1,) + cond_ctx.shape, bf16),
+            pltpu.VMEM((width // LANES, LANES), bf16),
+            pltpu.VMEM((1,) + query_gain.shape, bf16),
+            pltpu.VMEM((1,) + key_gain.shape, bf16),
+            pltpu.VMEM((offset_bias.shape[1], offset_bias.shape[0], offset_bias.shape[2]), f32),
             pltpu.VMEM((tokens, width), bf16),
-            pltpu.VMEM((halo, width), bf16),
-            pltpu.VMEM((halo, width), bf16),
+            pltpu.VMEM((2, halo, width), bf16),
             pltpu.VMEM((ctx_rows, width), bf16),
             pltpu.VMEM((3,) + shift_weight.shape, bf16),
             pltpu.VMEM(query_weight.shape, bf16),
@@ -1113,12 +1215,13 @@
             pltpu.VMEM((pairs, 2 * tokens, LANES), f32),
             pltpu.VMEM((pairs, 2 * tokens, 2 * LANES), f32),
             pltpu.VMEM((2, tokens, lane), bf16),
-            dma((9,)),
+            dma((15,)),
             dma((3,)), dma((3,)),
             dma((depth,)), dma((depth,)),
             dma((copies,)), dma((copies,)),
-            dma((2,)), dma((2,)),
-            dma((4 + pairs,)), dma((4 + pairs,)),
+            dma((reach,)), dma((reach,)),
+            dma((reach,)), dma((reach,)),
+            dma((swaps,)), dma((swaps,)),
         ],
         compiler_params=pltpu.CompilerParams(collective_id=0, has_side_effects=True),
         name="fused",

time: 61 us -> 42.8 us (0.70)
  the two profiles are of different devices: /device:TPU:3 before, /device:TPU:0 now
where the time goes in v2:
time: 42.8 us; the launch traced here: 42.7 us
  Pallas kernels  41.9 us (98%)
  local copies, waits for them, and re-layouts  0.8 us (2%)
    pallas_call x1, Pallas kernels, fused_body(): pl.pallas_call(functools.partial(fused_kernel, total_rows), out_shape=plt...  41.9 us

profile of v2, /device:TPU:0, one launch (start us, length us, event | category | flops | bytes accessed | tf_op | source)
XLA Modules:
  0.0 42.7 jit_solution(17162610963973852078)
XLA Ops:
  0.0 41.9 %fused.1 = bf16[256,1024]{1,0:T(8,128)(2,1)S(1)} custom-call(bf16[256,2048]{1,0:T(8,128)(2,1)} %latent_ref.1, bf16[32,2048]{1,0:T(8,128)(2,1)} %context_ref.1, bf16[1,128]{1,0:T(2,128)(2,1)} %bitcast.8, bf16[1,128]{1,0:T(2,128)(2,1)} %bitcast.9, bf16[128,1024]{1,0:T(8,128)(2,1)} %shift_ref.1, bf16[128,1024]{1,0:T(8,128)(2,1)} %scale_ref.1, ...), custom_call_target="tpu_custom_call" | custom-call | tf_op jit(solution)/shard_map/fused/pallas_call | solution.py:1181
  41.9 0.8 %copy.17 = bf16[256,1024]{1,0:T(8,128)(2,1)} copy(bf16[256,1024]{1,0:T(8,128)(2,1)S(1)} %fused.1) | data formatting | bytes 1048576

commit v3 on v2

--- a/solution.py
+++ b/solution.py
@@ -808,8 +808,7 @@
                     bound * LOG2E, (GRID_W, LANES)
                 )
 
-    quarter = pairs // 4
-    pl.loop(0, quarter)(bias_of)
+    early = pairs // 2
     pl.semaphore_wait(barrier, len(plane) + len(depth) + 3)
 
     first_stage = []
@@ -899,12 +898,11 @@
 
     near_masks = [mask for mask in depth if mask < size // 2]
     far_masks = [mask for mask in depth if mask >= size // 2][::-1]
-    via_x, via_y = far_masks[: len(far_masks) // 2], far_masks[len(far_masks) // 2 :]
     partner_copy(0).start()
     for mask in near_masks:
         ctx_start(0, mask)
 
-    pl.loop(quarter, 2 * quarter)(bias_of)
+    pl.loop(0, early)(bias_of)
     for copy in first_stage:
         copy.wait()
     total = sums[...]
@@ -918,6 +916,8 @@
         )
         copy.start()
         second_stage.append(copy)
+    for mask in far_masks:
+        ctx_start(0, mask)
     ctx_arrival(0, 1)
     ctx_start(1, 2)
     for mask in near_masks:
@@ -927,9 +927,7 @@
     for k in range(1, chunks):
         partner_copy(k).start()
 
-    pl.loop(2 * quarter, 3 * quarter)(bias_of)
-    relay(0)
-    pl.loop(3 * quarter, pairs)(bias_of)
+    pl.loop(early, pairs)(bias_of)
     for copy in second_stage:
         copy.wait()
     total = sums_z[...]
@@ -938,8 +936,7 @@
     final[0] = total
     swap = remote(final.at[0], final.at[1], tp_send.at[0], tp_recv.at[0], {"tp": other})
     swap.start()
-    for mask in far_masks:
-        ctx_start(0, mask)
+    relay(0)
     ctx_arrival(0, 2)
     ctx_arrival(1, 2)
     spread(ctx_x, plane_rows(0), plane_slot(0))
@@ -980,10 +977,12 @@
         inv = lax.rsqrt(jnp.mean(values * values, axis=-1, keepdims=True) + EPS)
         return (values * inv * (norm * (1.0 + scale)) + shift).astype(bf16)
 
-    def keys_values(hidden, k_out, v_out, at):
+    def keys_values(hidden, k_out, v_out, at, between=None):
         count = hidden.shape[0]
         raw = jnp.dot(hidden, wk[...], preferred_element_type=f32)
         k_out[pl.ds(at, count), :] = normed(raw, key_gain)
+        if between is not None:
+            between()
         raw = jnp.dot(hidden, wv[...], preferred_element_type=f32).astype(bf16)
         for p in range(pairs):
             v_out[pl.ds(at, count), 2 * p * LANES : (2 * p + 1) * LANES] = raw[
@@ -1002,13 +1001,11 @@
         ctx_arrival(mask, 2)
         ctx_arrival(mask ^ 1, 2)
         spread(ctx_x, plane_rows(mask), plane_slot(mask))
+    relay(2)
     for mask in [0] + near_masks:
         finish(ctx_x, plane_rows(mask), plane_slot(mask))
 
-    def between(far):
-        if far:
-            return
-        relay(2)
+    def far_on():
         for mask in far_masks:
             ctx_arrival(0, mask)
             ctx_start(mask, 1)
@@ -1020,11 +1017,14 @@
             index = 1 - index
         at = pl.multiple_of(index * half_ctx, half_ctx)
         hidden = hidden_of(ctx_x[pl.ds(at, half_ctx), :], shift_ctx, scale_ctx)
-        between(far)
-        keys_values(hidden, ck_buf, cv_buf, at)
+        keys_values(hidden, ck_buf, cv_buf, at, None if far else far_on)
         return pl.ds(at, half_ctx)
 
     near_rows = ctx_half(False)
+    for k in range(3, chunks):
+        relay(k)
+    for mask in far_masks:
+        ctx_start(mask, 2)
 
     contract = (((1,), (1,)), ((), ()))
 
@@ -1045,14 +1045,9 @@
         weight = jnp.exp2(score - shown).astype(bf16)
         return jnp.dot(weight, cv_buf[rows, at2], preferred_element_type=f32)
 
-    @pl.loop(0, pairs)
-    def _(pair):
+    for pair in range(pairs):
         near[pair] = from_ctx(pair, near_rows)
 
-    for k in range(3, chunks):
-        relay(k)
-    for mask in far_masks:
-        ctx_start(mask, 2)
     for k in range(chunks):
         finish(halo_x.at[1 - parity], pl.ds(k * step, step), 1 + k)
     stride = halo + tokens
@@ -1060,7 +1055,7 @@
         hidden_of(halo_x[1 - parity], shift, scale),
         k_buf, v_buf, pl.multiple_of((1 - parity) * stride, stride),
     )
-    for mask in via_y:
+    for mask in far_masks:
         ctx_arrival(mask, 1)
         ctx_start(mask ^ 1, 2)
 
@@ -1069,10 +1064,6 @@
         for k in range(chunks):
             relay_copy(k).wait_recv()
             spread(halo_x.at[parity], pl.ds(k * step, step), 1 + chunks + k)
-
-    for mask in via_x:
-        ctx_arrival(mask, 2)
-        ctx_start(mask ^ 2, 1)
 
     @pl.when(has_behind)
     def _():
@@ -1102,10 +1093,7 @@
             near[pair, tokens + row * GRID_W : tokens + (row + 1) * GRID_W, :] += acc[GRID_W:]
 
     pl.loop(0, pairs // 2)(from_window)
-    for mask in via_x:
-        ctx_arrival(mask, 1)
-        ctx_arrival(mask ^ 2, 1)
-    for mask in via_y:
+    for mask in far_masks:
         ctx_arrival(mask, 2)
         ctx_arrival(mask ^ 1, 2)
     for mask in far_masks:
@@ -1125,9 +1113,8 @@
             tp_send.at[mix_slot + pair], tp_recv.at[mix_slot + pair], {"tp": other},
         )
 
-    @pl.loop(0, pairs)
-    def _(pair):
-        at = pl.ds(pl.multiple_of(pair * LANES, LANES), LANES)
+    for pair in range(pairs):
+        at = slice(pair * LANES, (pair + 1) * LANES)
         acc = near[pair] + from_ctx(pair, far_rows)
         mixed = acc[:, :LANES] / acc[:, LANES:]
         left = lax.broadcasted_iota(jnp.int32, (tokens, LANES), 1) < HEAD_DIM
@@ -1138,10 +1125,16 @@
     out = jnp.dot(
         mix[0], wo[pl.ds(pl.multiple_of(mine * lane, lane), lane), :], preferred_element_type=f32
     )
-    for pair in range(pairs):
+    begin = pl.multiple_of(other * lane, lane)
+    most = lane - LANES
+    for pair in range(pairs - 1):
         mix_copy(pair).wait()
     out = out + jnp.dot(
-        mix[1], wo[pl.ds(pl.multiple_of(other * lane, lane), lane), :], preferred_element_type=f32
+        mix[1, :, :most], wo[pl.ds(begin, most), :], preferred_element_type=f32
+    )
+    mix_copy(pairs - 1).wait()
+    out = out + jnp.dot(
+        mix[1, :, most:], wo[pl.ds(begin + most, LANES), :], preferred_element_type=f32
     )
     out_ref[...] = (own_x[:, cols].astype(f32) + mod[4:5, cols] * out).astype(bf16)
 

time: 42.8 us -> 41.1 us (0.960)
  the two profiles are of different devices: /device:TPU:0 before, /device:TPU:3 now
where the time goes in v3:
time: 41.1 us; the launch traced here: 40.4 us
  Pallas kernels  39.6 us (96%)
  local copies, waits for them, and re-layouts  0.8 us (2%)
    pallas_call x1, Pallas kernels, fused_body(): pl.pallas_call(functools.partial(fused_kernel, total_rows), out_shape=plt...  39.6 us

profile of v3, /device:TPU:3, one launch (start us, length us, event | category | flops | bytes accessed | tf_op | source)
XLA Modules:
  0.0 40.4 jit_solution(6556692479885581640)
XLA Ops:
  0.0 39.6 %fused.1 = bf16[256,1024]{1,0:T(8,128)(2,1)S(1)} custom-call(bf16[256,2048]{1,0:T(8,128)(2,1)} %latent_ref.1, bf16[32,2048]{1,0:T(8,128)(2,1)} %context_ref.1, bf16[1,128]{1,0:T(2,128)(2,1)} %bitcast.8, bf16[1,128]{1,0:T(2,128)(2,1)} %bitcast.9, bf16[128,1024]{1,0:T(8,128)(2,1)} %shift_ref.1, bf16[128,1024]{1,0:T(8,128)(2,1)} %scale_ref.1, ...), custom_call_target="tpu_custom_call" | custom-call | tf_op jit(solution)/shard_map/fused/pallas_call | solution.py:1174
  39.6 0.8 %copy.17 = bf16[256,1024]{1,0:T(8,128)(2,1)} copy(bf16[256,1024]{1,0:T(8,128)(2,1)S(1)} %fused.1) | data formatting | bytes 1048576
